TPU v7x, 32 devices: a whole 2x2x4 slice. The times are simulated.
32 devices in a mesh: ep: 8 (over z, y), tp: 4 (over x, core).
Axes of the slice: x: 2, y: 2, z: 4, core: 2. Of those that a mesh axis runs over, the one named last changes fastest.
Arguments:
- mixer_input: bfloat16 [4096, 2048], P('ep'), may hold values from -6 to 6
- log_forget_total: float32 [16, 4096], P('tp'), may hold values from -684 to 0, as said below
- mixer_gain: float32 [2048], replicated, may hold values from 0.1 to 1.9
- w_query: bfloat16 [2048, 1024], P(None, 'tp'), may hold values from -1 to 1
- w_key: bfloat16 [2048, 256], P(None, 'tp'), may hold values from -8 to 8
- w_value: bfloat16 [2048, 256], P(None, 'tp'), may hold values from -0.125 to 0.125
- w_output: bfloat16 [1024, 2048], replicated, may hold values from -0.1875 to 0.1875
- mixer_post_gain: float32 [2048], replicated, may hold values from 0.1 to 1.9
- expert_input: bfloat16 [2048, 2048], P('ep'), may hold values from -6 to 6
- expert_ids: int32 [2048, 2], P('ep'), may hold values from 0 to 7, all different within a row; in each aligned block of 64 rows (0 to 63, 64 to 127, ...) at most 32 rows name the same one
- route_weight: float32 [2048, 2], P('ep'), may hold values from 0.1 to 1
- expert_gain: float32 [2048], replicated, may hold values from 0.1 to 1.9
- w_gate: bfloat16 [8, 2048, 3584], P('ep', None, 'tp'), may hold values from -0.125 to 0.125
- w_up: bfloat16 [8, 2048, 3584], P('ep', None, 'tp'), may hold values from -0.125 to 0.125
- w_down: bfloat16 [8, 3584, 2048], P('ep', 'tp'), may hold values from -0.09375 to 0.09375
- expert_post_gain: float32 [2048], replicated, may hold values from 0.1 to 1.9
Outputs:
- mixer_out: bfloat16 [4096, 2048], P(('ep', 'tp'))
- expert_out: bfloat16 [2048, 2048], P(('ep', 'tp'))
Inputs may be any that keep to these rules, and one draw needn't show every extreme that they name: `expert_ids`: in each aligned block of 64 tokens no expert is named by more than 32 of them. `log_forget_total`: each head's values never rise along the positions.
All inputs are finite; a program needn't handle non-finite values.
Results may differ from a plain program's by a relative error of at most 0.012.
The roundings to bfloat16 on the way count: a program that leaves them out, or rounds other values in their place, can miss the bound.
Values may be sent and summed in bfloat16 or wider, within the bound.
A program may use at most 128 MiB of HBM per device.

v0:
```python
import functools

import jax
import jax.numpy as jnp
from jax import lax
from jax.experimental import pallas as pl
from jax.experimental.pallas import tpu as pltpu
from jax.sharding import PartitionSpec as P

HD = 64
TOP_K = 2


NEG_FILL = -1e30
NORM_EPS = 1e-06


def norm_rows(values_in, gain_vec):
    widened = values_in.astype(jnp.float32)
    return (
        widened
        * lax.rsqrt(jnp.mean(widened * widened, axis=-1, keepdims=True) + NORM_EPS)
        * gain_vec
    )


def meet(axis_sizes):
    barrier = pltpu.get_barrier_semaphore()
    for axis, size in axis_sizes:
        place = lax.axis_index(axis)
        for step in range(1, size):
            pl.semaphore_signal(
                barrier,
                inc=1,
                device_id={axis: lax.rem(place + step, size)},
                device_id_type=pl.DeviceIdType.MESH,
            )
    pl.semaphore_wait(barrier, sum(size - 1 for _, size in axis_sizes))


def push(source, target, sems, index, axis, place):
    return pltpu.make_async_remote_copy(
        src_ref=source,
        dst_ref=target,
        send_sem=sems.at[0, index],
        recv_sem=sems.at[1, index],
        device_id={axis: place},
        device_id_type=pl.DeviceIdType.MESH,
    )


def inward_kernel(
    n_ep, rows, heads, q_ref, kv_ref, gate_ref, out_rows, mixed_ref, slots_ref,
    kv_all, max_ref, acc_ref, kv_sem, f_sem, ep_sem, x_sem, c_sem, d_sem,
):
    own = lax.axis_index("ep")
    quarter = lax.axis_index("tp")
    across = lax.rem(quarter + 2, 4)
    beside = quarter + 1 - 2 * lax.rem(quarter, 2)
    max_ref[...] = jnp.full(max_ref.shape, NEG_FILL, jnp.float32)
    acc_ref[...] = jnp.zeros(acc_ref.shape, jnp.float32)
    meet((("ep", n_ep), ("tp", 4)))

    def block(kv, index, diagonal):
        first = pl.multiple_of(index * rows, rows)
        keys = kv[:, :HD]
        lane = lax.broadcasted_iota(jnp.int32, kv.shape, 1)
        values = jnp.where(lane < HD, jnp.ones_like(kv), kv)
        gates = gate_ref[:, pl.ds(first, rows)]
        for head in range(heads):
            scores = lax.dot_general(
                q_ref[head], keys, (((1,), (1,)), ((), ())), preferred_element_type=jnp.float32
            )
            scores = scores - gates[head : head + 1, :]
            if diagonal:
                row = lax.broadcasted_iota(jnp.int32, scores.shape, 0)
                column = lax.broadcasted_iota(jnp.int32, scores.shape, 1)
                scores = jnp.where(column <= row, scores, NEG_FILL)
            old_max = max_ref[head][:, :1]
            new_max = jnp.maximum(old_max, jnp.max(scores, axis=1, keepdims=True))
            shifted = jnp.exp(scores - new_max).astype(jnp.bfloat16)
            acc_ref[head] = acc_ref[head] * jnp.exp(old_max - new_max) + jnp.dot(
                shifted, values, preferred_element_type=jnp.float32
            )
            max_ref[head] = jnp.broadcast_to(new_max, max_ref.shape[1:])

    def kv_copy(source, place):
        return push(kv_ref, kv_all.at[source], kv_sem, source, "ep", place)

    def ep_copy(source, place):
        return pltpu.make_async_remote_copy(
            src_ref=out_rows.at[place],
            dst_ref=slots_ref.at[quarter, source],
            send_sem=ep_sem.at[0, place],
            recv_sem=ep_sem.at[1, source],
            device_id={"ep": place},
            device_id_type=pl.DeviceIdType.MESH,
        )

    def kv_send(place):
        return pltpu.make_async_remote_copy(
            src_ref=kv_ref,
            dst_ref=kv_all.at[own],
            send_sem=kv_sem.at[0, place],
            recv_sem=kv_sem.at[1, own],
            device_id={"ep": place},
            device_id_type=pl.DeviceIdType.MESH,
        )

    def to_across(source, held):
        return push(held, slots_ref.at[quarter, source], x_sem, source, "tp", across)

    def to_beside(source, held):
        return push(held, slots_ref.at[quarter, source], c_sem, source, "tp", beside)

    def second(source):
        held = slots_ref.at[across, source]
        return push(held, slots_ref.at[across, source], d_sem, source, "tp", beside)

    odd = lax.rem(own, 2)
    partner = own + 1 - 2 * odd

    def sends_to(step):
        reaches = (lax.rem(step, 2) == 0) | ((step == 1) & (odd == 0))
        return (step > 0) & reaches & (own + step < n_ep)

    def hands_on(step):
        return (step > 0) & (lax.rem(step, 2) == 0) & (step <= own)

    def hand_on(step):
        source = own - step
        return push(kv_all.at[source], kv_all.at[source], f_sem, source, "ep", partner)

    def send(step, carry):
        @pl.when(sends_to(step))
        def _():
            kv_send(own + step).start()

        ep_copy(own, lax.rem(own + step, n_ep)).start()
        return carry

    lax.fori_loop(1, n_ep, send, 0)
    to_across(own, out_rows.at[own]).start()
    to_beside(own, out_rows.at[own]).start()
    slots_ref[quarter, own] = out_rows[own]
    block(kv_ref[...], own, True)

    def work(step, carry):
        @pl.when(hands_on(step + 1))
        def _():
            kv_copy(own - step - 1, own).wait_recv()
            hand_on(step + 1).start()

        @pl.when((step <= own) & (lax.rem(step, 2) == 1))
        def _():
            from_partner = (step == 1) & (odd == 1)

            @pl.when(from_partner)
            def _():
                kv_copy(own - step, own).wait_recv()

            @pl.when(jnp.logical_not(from_partner))
            def _():
                hand_on(step).wait_recv()

        @pl.when(step <= own)
        def _():
            block(kv_all[own - step], own - step, False)

        source = lax.rem(own - step + n_ep, n_ep)
        ep_copy(source, source).wait_recv()
        held = slots_ref.at[quarter, source]
        to_across(source, held).start()
        to_beside(source, held).start()
        earlier = lax.rem(own - step + 1 + n_ep, n_ep)
        to_across(earlier, slots_ref.at[across, earlier]).wait_recv()
        second(earlier).start()
        return carry

    lax.fori_loop(1, n_ep, work, 0)
    last = lax.rem(own + 1, n_ep)
    to_across(last, slots_ref.at[across, last]).wait_recv()
    second(last).start()
    for head in range(heads):
        total = acc_ref[head]
        mixed_ref[head] = (total[:, HD:] / total[:, :HD]).astype(mixed_ref.dtype)

    def drain(step, carry):
        place = lax.rem(own + step, n_ep)

        @pl.when(sends_to(step))
        def _():
            kv_send(own + step).wait_send()

        @pl.when(hands_on(step))
        def _():
            hand_on(step).wait_send()

        @pl.when(step > 0)
        def _():
            ep_copy(own, place).wait_send()

        to_across(place, out_rows.at[own]).wait_send()
        to_beside(place, out_rows.at[own]).wait()
        second(place).wait()
        return carry

    lax.fori_loop(0, n_ep, drain, 0)


def inward(queries, kv_rows, gate_totals, outgoing):
    heads, rows, _ = queries.shape
    n_ep, slot_count, width = outgoing.shape
    pair = pltpu.SemaphoreType.DMA((2, n_ep))
    return pl.pallas_call(
        functools.partial(inward_kernel, n_ep, rows, heads),
        out_shape=(
            jax.ShapeDtypeStruct(queries.shape, jnp.bfloat16),
            jax.ShapeDtypeStruct((4, n_ep, slot_count, width), jnp.bfloat16),
        ),
        in_specs=[pl.BlockSpec(memory_space=pltpu.VMEM)] * 4,
        out_specs=[pl.BlockSpec(memory_space=pltpu.VMEM)] * 2,
        scratch_shapes=[
            pltpu.VMEM((n_ep, rows, 2 * HD), jnp.bfloat16),
            pltpu.VMEM((heads, rows, 2 * HD), jnp.float32),
            pltpu.VMEM((heads, rows, 2 * HD), jnp.float32),
            pair, pair, pair, pair, pair, pair,
        ],
        compiler_params=pltpu.CompilerParams(
            collective_id=0, has_side_effects=True, vmem_limit_bytes=40 * 1024 * 1024
        ),
    )(queries, kv_rows, gate_totals, outgoing)


def outward_kernel(
    n_ep, product_ref, mixed_ref, heads_ref, result_ref,
    arrived, summed, crossed, final, h_sem, p_sem, r_sem, x_sem, ep_sem,
):
    own = lax.axis_index("ep")
    quarter = lax.axis_index("tp")
    across = lax.rem(quarter + 2, 4)
    beside = quarter + 1 - 2 * lax.rem(quarter, 2)
    diagonal = lax.rem(beside + 2, 4)
    meet((("ep", n_ep), ("tp", 4)))

    def heads_copy(step):
        place = lax.rem(quarter + step, 4)
        return pltpu.make_async_remote_copy(
            src_ref=mixed_ref.at[place],
            dst_ref=heads_ref.at[quarter],
            send_sem=h_sem.at[0, step],
            recv_sem=h_sem.at[1, step],
            device_id={"tp": place},
            device_id_type=pl.DeviceIdType.MESH,
        )

    def near(j):
        return push(product_ref.at[beside, j], arrived.at[0, j], p_sem, j, "tp", beside)

    def far(j):
        return push(product_ref.at[diagonal, j], arrived.at[1, j], r_sem, j, "tp", beside)

    def cross(j):
        return push(summed.at[j], crossed.at[j], x_sem, j, "tp", across)

    def home(j, source):
        return pltpu.make_async_remote_copy(
            src_ref=final.at[j],
            dst_ref=result_ref.at[source],
            send_sem=ep_sem.at[0, j],
            recv_sem=ep_sem.at[1, source],
            device_id={"ep": j},
            device_id_type=pl.DeviceIdType.MESH,
        )

    def begin(step, carry):
        j = lax.rem(own + step, n_ep)
        far(j).start()
        near(j).start()
        return carry

    lax.fori_loop(1, n_ep + 1, begin, 0)
    for step in range(1, 4):
        heads_copy(step).start()
    heads_ref[quarter] = mixed_ref[quarter]

    def pair_sum(step, carry):
        j = lax.rem(own + step, n_ep)
        far(j).wait_recv()
        total = product_ref[across, j].astype(jnp.float32) + arrived[1, j].astype(jnp.float32)
        summed[j] = total.astype(jnp.bfloat16)
        cross(j).start()
        return carry

    lax.fori_loop(1, n_ep + 1, pair_sum, 0)

    def finish(j):
        near(j).wait_recv()
        cross(j).wait_recv()
        total = product_ref[quarter, j].astype(jnp.float32) + arrived[0, j].astype(jnp.float32)
        return (total + crossed[j].astype(jnp.float32)).astype(jnp.bfloat16)

    def full_sum(step, carry):
        j = lax.rem(own + step, n_ep)
        final[j] = finish(j)
        home(j, own).start()
        return carry

    lax.fori_loop(1, n_ep, full_sum, 0)
    result_ref[own] = finish(own)
    for step in range(1, 4):
        heads_copy(step).wait()

    def drain(step, carry):
        j = lax.rem(own + step, n_ep)
        near(j).wait_send()
        far(j).wait_send()
        cross(j).wait_send()

        @pl.when(step < n_ep)
        def _():
            home(j, own).wait_send()
            home(j, j).wait_recv()

        return carry

    lax.fori_loop(1, n_ep + 1, drain, 0)


def outward(product, mixed):
    _, n_ep, slot_count, width = product.shape
    pair = pltpu.SemaphoreType.DMA((2, n_ep))
    chunk = (n_ep, slot_count, width)
    return pl.pallas_call(
        functools.partial(outward_kernel, n_ep),
        out_shape=(
            jax.ShapeDtypeStruct(mixed.shape, jnp.bfloat16),
            jax.ShapeDtypeStruct(chunk, jnp.bfloat16),
        ),
        in_specs=[pl.BlockSpec(memory_space=pltpu.VMEM)] * 2,
        out_specs=[pl.BlockSpec(memory_space=pltpu.VMEM)] * 2,
        scratch_shapes=[
            pltpu.VMEM((2,) + chunk, jnp.bfloat16),
            pltpu.VMEM(chunk, jnp.bfloat16),
            pltpu.VMEM(chunk, jnp.bfloat16),
            pltpu.VMEM(chunk, jnp.bfloat16),
            pltpu.SemaphoreType.DMA((2, 4)),
            pair, pair, pair, pair,
        ],
        compiler_params=pltpu.CompilerParams(
            collective_id=1, has_side_effects=True, vmem_limit_bytes=40 * 1024 * 1024
        ),
    )(product, mixed)


def attention_inputs(mixer_input, mixer_gain, w_query, w_key, w_value):
    row_count = mixer_input.shape[0]
    head_local = w_query.shape[1] // HD
    normed = norm_rows(mixer_input, mixer_gain).astype(jnp.bfloat16)
    w_kv = jnp.concatenate([w_key, w_value], axis=1)
    kv_rows = jnp.dot(normed, w_kv, preferred_element_type=jnp.float32).astype(jnp.bfloat16)
    queries = jnp.dot(normed, w_query, preferred_element_type=jnp.float32).astype(jnp.bfloat16)
    queries = queries * jnp.bfloat16(HD ** (-0.5))
    queries = jnp.transpose(queries.reshape(row_count, head_local, HD), (1, 0, 2))
    return queries, kv_rows


def routed_rows(expert_input, expert_ids, route_weight, expert_gain):
    row_count = expert_input.shape[0]
    quarters = lax.axis_size("tp")
    experts = lax.axis_size("ep")
    quarter_rows = row_count // quarters
    slot_count = 2 * TOP_K * quarter_rows // experts
    first = lax.axis_index("tp") * quarter_rows
    own_input = lax.dynamic_slice_in_dim(expert_input, first, quarter_rows, 0)
    own_weights = lax.dynamic_slice_in_dim(route_weight, first, quarter_rows, 0)
    routed = lax.dynamic_slice_in_dim(expert_ids, first, quarter_rows, 0)
    normed = norm_rows(own_input, expert_gain).astype(jnp.bfloat16)
    matches = routed[:, :, None] == jnp.arange(experts, dtype=jnp.int32)[None, None, :]
    matches = matches.astype(jnp.bfloat16)
    per_token = jnp.sum(matches, axis=1)
    position = jnp.arange(quarter_rows, dtype=jnp.int32)
    lower = (position[None, :] < position[:, None]).astype(jnp.bfloat16)
    before = jnp.dot(lower, per_token, preferred_element_type=jnp.float32)
    ranks = jnp.sum(matches.astype(jnp.float32) * before[:, None, :], axis=2).astype(jnp.int32)
    slots = routed * slot_count + ranks
    total_slots = experts * slot_count
    chosen = slots[:, :, None] == jnp.arange(total_slots, dtype=jnp.int32)[None, None, :]
    chosen = chosen.astype(jnp.bfloat16)
    outgoing = lax.dot_general(
        jnp.sum(chosen, axis=1), normed, (((0,), (0,)), ((), ())),
        preferred_element_type=jnp.float32,
    ).astype(jnp.bfloat16)
    return outgoing.reshape(experts, slot_count, -1), chosen, own_weights


def per_device(
    mixer_input,
    log_forget_total,
    mixer_gain,
    w_query,
    w_key,
    w_value,
    w_output,
    mixer_post_gain,
    expert_input,
    expert_ids,
    route_weight,
    expert_gain,
    w_gate,
    w_up,
    w_down,
    expert_post_gain,
):
    queries, kv_rows = attention_inputs(mixer_input, mixer_gain, w_query, w_key, w_value)
    outgoing, chosen, own_weights = routed_rows(
        expert_input, expert_ids, route_weight, expert_gain
    )
    mixed, slot_rows = inward(queries, kv_rows, log_forget_total, outgoing)
    flat_rows = slot_rows.reshape(-1, slot_rows.shape[-1])
    gate_part = jnp.dot(flat_rows, w_gate[0], preferred_element_type=jnp.float32)
    up_part = jnp.dot(flat_rows, w_up[0], preferred_element_type=jnp.float32)
    hidden = (jax.nn.silu(gate_part) * up_part).astype(jnp.bfloat16)
    product = jnp.dot(hidden, w_down[0], preferred_element_type=jnp.float32).astype(jnp.bfloat16)
    quarters = slot_rows.shape[0]
    heads, rows, _ = mixed.shape
    mixed_heads = jnp.transpose(mixed, (1, 0, 2)).reshape(quarters, rows // quarters, heads * HD)
    head_rows, returned = outward(product.reshape(slot_rows.shape), mixed_heads)
    by_rows = jnp.transpose(head_rows, (1, 0, 2)).reshape(rows // quarters, -1)
    projected = jnp.dot(by_rows, w_output, preferred_element_type=jnp.float32)
    mixer_out = norm_rows(projected, mixer_post_gain).astype(jnp.bfloat16)
    returned = returned.reshape(-1, returned.shape[-1])
    combined = 0.0
    for k in range(TOP_K):
        picked = jnp.dot(chosen[:, k], returned, preferred_element_type=jnp.float32)
        combined = combined + own_weights[:, k : k + 1] * picked
    expert_out = norm_rows(combined, expert_post_gain).astype(jnp.bfloat16)
    return (mixer_out, expert_out)


def solution(mesh):
    placed = (
        P("ep", None),
        P("tp", None),
        P(),
        P(None, "tp"),
        P(None, "tp"),
        P(None, "tp"),
        P(),
        P(),
        P("ep", None),
        P("ep", None),
        P("ep", None),
        P(),
        P("ep", None, "tp"),
        P("ep", None, "tp"),
        P("ep", "tp", None),
        P(),
    )
    return jax.shard_map(
        per_device,
        mesh=mesh,
        in_specs=placed,
        out_specs=(P(("ep", "tp"), None), P(("ep", "tp"), None)),
        check_vma=False,
    )
```

profile of v0, /device:TPU:17, one launch (start us, length us, event | category | flops | bytes accessed | tf_op | source)
XLA Modules:
  0.0 136.0 jit_solution(15861599754188599433)
XLA Ops:
  0.6 1.2 fusion.14
  1.9 0.8 constant_dynamic-slice_fusion.1
  2.6 0.7 constant_dynamic-slice_fusion
  3.5 0.8 convert_add_fusion
  4.3 2.2 %fusion = f32[512]{0:T(512)S(1)} fusion(bf16[512,2048]{1,0:T(8,128)(2,1)} %param.16), kind=kLoop, calls=%fused_computation.2 | loop fusion | flops 3145216 | bytes 2099200 | tf_op jit(solution)/shard_map/reduce_sum | solution.py:22
  6.7 2.4 %convolution_convert_fusion.3.kv_ref = bf16[512,128]{1,0:T(8,128)(2,1)S(1)} fusion(bf16[512,2048]{1,0:T(8,128)(2,1)} %param.16, f32[2048]{0:T(1024)} %param.18, f32[512]{0:T(512)S(1)} %add_rsqrt_fusion, bf16[2048,64]{0,1:T(8,128)(2,1)} %param.21, bf16[2048,64]{0,1:T(8,128)(2,1)} %param.20), kind=kOutput, calls=%fused_computation.18 | convolution fusion | flops 273743872 | bytes 2762752 | tf_op jit(solution)/shard_map/dot_general | solution.py:361
  9.2 0.9 fusion.11
  10.2 0.3 copy.28
  10.5 1.4 %convolution_convert_fusion.1 = bf16[256,2048]{1,0:T(8,128)(2,1)S(1)} fusion(bf16[64,256]{1,0:T(8,128)(2,1)S(1)} %convert_reduce_fusion, f32[2048]{0:T(1024)S(1)} %copy-done.6, f32[64]{0:T(128)S(1)} %add_rsqrt_fusion.3, bf16[256,2048]{1,0:T(8,128)(2,1)} %param.24, s32[]{:T(128)S(6)} %select_n.2), kind=kOutput, calls=%fused_computation.12 | convolution fusion | flops 68157440 | bytes 1351940 | tf_op jit(solution)/shard_map/dot_general | solution.py:390
  11.9 53.1 %shard_map.167 = (bf16[4,512,64]{2,1,0:T(8,128)(2,1)S(1)}, bf16[4,8,32,2048]{3,2,1,0:T(8,128)(2,1)S(1)}) custom-call(bf16[4,512,64]{2,1,0:T(8,128)(2,1)S(1)} %bitcast.46, bf16[512,128]{1,0:T(8,128)(2,1)S(1)} %convolution_convert_fusion.3.kv_ref, f32[4,4096]{1,0:T(4,128)S(1)} %copy-done.1, bf16[8,32,2048]{2,1,0:T(8,128)(2,1)S(1)} %bitcast.42), custom_call_target="tpu_custom_call" | custom-call | tf_op jit(solution)/shard_map/pallas_call | solution.py:215
  65.0 1.9 %copy-done.2 = bf16[4,8,32,2048]{3,2,1,0:T(8,128)(2,1)} copy-done((bf16[4,8,32,2048]{3,2,1,0:T(8,128)(2,1)}, bf16[4,8,32,2048]{3,2,1,0:T(8,128)(2,1)S(1)}, u32[]{:S(2)}) %copy-start.2) | copy-done | bytes 4194328
  66.9 0.4 copy.32
  67.3 0.3 reshape.71.mixed_ref
  67.7 7.5 %fusion.4 = f32[1024,896]{1,0:T(8,128)S(1)} fusion(bf16[1024,2048]{1,0:T(8,128)(2,1)} %bitcast.49, bf16[1,2048,896]{2,1,0:T(8,128)(2,1)} %param.29), kind=kOutput, calls=%fused_computation.7 | convolution fusion | flops 3758096384 | bytes 11534336 | tf_op jit(solution)/shard_map/dot_general | solution.py:422
  75.2 4.8 %multiply_convert_fusion = bf16[1024,896]{1,0:T(8,128)(2,1)S(1)} fusion(f32[1024,896]{1,0:T(8,128)S(1)} %fusion.4, bf16[1024,2048]{1,0:T(8,128)(2,1)S(1)} %bitcast.50, bf16[1,2048,896]{2,1,0:T(8,128)(2,1)S(1)} %copy-done.9), kind=kOutput, calls=%fused_computation.11 | convolution fusion | flops 3763601408 | bytes 13369344 | tf_op jit(solution)/shard_map/dot_general | solution.py:421
  80.0 4.9 %convolution_convert_fusion = bf16[1024,2048]{1,0:T(8,128)(2,1)S(1)} fusion(bf16[1024,896]{1,0:T(8,128)(2,1)S(1)} %multiply_convert_fusion, bf16[1,896,2048]{2,1,0:T(8,128)(2,1)S(1)} %copy-done.10), kind=kOutput, calls=%fused_computation.5 | convolution fusion | flops 3760193536 | bytes 9699328 | tf_op jit(solution)/shard_map/dot_general | solution.py:424
  85.0 46.7 %shard_map.168 = (bf16[4,128,256]{2,1,0:T(8,128)(2,1)S(1)}, bf16[8,32,2048]{2,1,0:T(8,128)(2,1)S(1)}) custom-call(bf16[4,8,32,2048]{3,2,1,0:T(8,128)(2,1)S(1)} %bitcast.43, bf16[4,128,256]{2,1,0:T(8,128)(2,1)S(1)} %reshape.71.mixed_ref), custom_call_target="tpu_custom_call" | custom-call | tf_op jit(solution)/shard_map/pallas_call | solution.py:334
  131.7 0.2 copy.31
  131.9 0.3 convolution_multiply_fusion.1
  132.2 0.4 multiply_reduce_fusion.1
  132.7 0.8 multiply_convert_fusion.2
  133.5 0.7 copy-done.4
  134.2 0.8 multiply_reduce_fusion
  135.0 1.0 multiply_convert_fusion.1
  (32 shorter events, 0.4 us)
Async XLA Ops:
  0.6 8.5 %copy-start = (bf16[2048,256]{1,0:T(8,128)(2,1)S(1)}, bf16[2048,256]{1,0:T(8,128)(2,1)}, u32[]{:S(2)}) copy-start(bf16[2048,256]{1,0:T(8,128)(2,1)} %param.19) | copy-start | bytes 3145732
  4.3 4.9 %copy-start.5 = (bf16[512,2048]{1,0:T(8,128)(2,1)S(1)}, bf16[512,2048]{1,0:T(8,128)(2,1)}, u32[]{:S(2)}) copy-start(bf16[512,2048]{1,0:T(8,128)(2,1)} %param.16) | copy-start | bytes 6291460
  4.3 4.9 %copy-start.11 = (f32[2048]{0:T(1024)S(1)}, f32[2048]{0:T(1024)}, u32[]{:S(2)}) copy-start(f32[2048]{0:T(1024)} %param.18) | copy-start | bytes 24580
  9.2 1.3 copy-start.6
  9.2 2.7 %copy-start.1 = (f32[4,4096]{1,0:T(4,128)S(1)}, f32[4,4096]{1,0:T(4,128)}, u32[]{:S(2)}) copy-start(f32[4,4096]{1,0:T(4,128)} %gate_ref.1) | copy-start | bytes 196612
  65.0 1.9 %copy-start.2 = (bf16[4,8,32,2048]{3,2,1,0:T(8,128)(2,1)}, bf16[4,8,32,2048]{3,2,1,0:T(8,128)(2,1)S(1)}, u32[]{:S(2)}) copy-start(bf16[4,8,32,2048]{3,2,1,0:T(8,128)(2,1)S(1)} %get-tuple-element.6) | copy-start | bytes 12582916
  67.7 7.5 %copy-start.3 = (bf16[4,8,32,2048]{3,2,1,0:T(8,128)(2,1)S(1)}, bf16[4,8,32,2048]{3,2,1,0:T(8,128)(2,1)}, u32[]{:S(2)}) copy-start(bf16[4,8,32,2048]{3,2,1,0:T(8,128)(2,1)} %copy-done.2) | copy-start | bytes 12582916
  67.7 7.5 %copy-start.9 = (bf16[1,2048,896]{2,1,0:T(8,128)(2,1)S(1)}, bf16[1,2048,896]{2,1,0:T(8,128)(2,1)}, u32[]{:S(2)}) copy-start(bf16[1,2048,896]{2,1,0:T(8,128)(2,1)} %param.28) | copy-start | bytes 11010052
  75.2 4.8 %copy-start.10 = (bf16[1,896,2048]{2,1,0:T(8,128)(2,1)S(1)}, bf16[1,896,2048]{2,1,0:T(8,128)(2,1)}, u32[]{:S(2)}) copy-start(bf16[1,896,2048]{2,1,0:T(8,128)(2,1)} %param.30) | copy-start | bytes 11010052
  84.9 47.7 %copy-start.7 = (f32[2048]{0:T(1024)S(1)}, f32[2048]{0:T(1024)}, u32[]{:S(2)}) copy-start(f32[2048]{0:T(1024)} %param.31) | copy-start | bytes 24580
  131.9 2.3 %copy-start.4 = (bf16[1024,2048]{1,0:T(8,128)(2,1)S(1)}, bf16[1024,2048]{1,0:T(8,128)(2,1)}, u32[]{:S(2)}) copy-start(bf16[1024,2048]{1,0:T(8,128)(2,1)} %param.22) | copy-start | bytes 12582916
  132.6 2.4 %copy-start.8 = (f32[2048]{0:T(1024)S(1)}, f32[2048]{0:T(1024)}, u32[]{:S(2)}) copy-start(f32[2048]{0:T(1024)} %param.23) | copy-start | bytes 24580
where the time goes:
time: 138 us; the launch traced here: 136 us
  Pallas kernels  99.8 us (72%)
  matrix products  23.7 us (17%)
  other arithmetic  6.18 us (4%)
  local copies, waits for them, and re-layouts  5.4 us (4%)
    pallas_call x1, Pallas kernels, inward(): pl.pallas_call(functools.partial(inward_kernel, n_ep, rows, heads), out_s...  53.1 us
    pallas_call x1, Pallas kernels, outward(): pl.pallas_call(functools.partial(outward_kernel, n_ep), out_shape=(jax.Sh...  46.7 us
    dot_general x1, matrix products, per_device(): up_part = jnp.dot(flat_rows, w_up[0], preferred_element_type=jnp.float32)  7.5 us
    dot_general x1, matrix products, per_device(): jnp.dot(hidden, w_down[0], preferred_element_type=jnp.float32)  4.93 us
    dot_general x1, matrix products, per_device(): jnp.dot(flat_rows, w_gate[0], preferred_element_type=jnp.float32)  4.75 us
    reduce_sum x2, other arithmetic, norm_rows(): jnp.mean(widened * widened, axis=-1, keepdims=True) + NORM_EPS  3.41 us

commit v1 on v0

v1 whole, which is shorter than its diff:
```python
import functools

import jax
import jax.numpy as jnp
from jax import lax
from jax.experimental import pallas as pl
from jax.experimental.pallas import tpu as pltpu
from jax.sharding import PartitionSpec as P

HD = 64
TOP_K = 2
ONES = 16
LOG2E = 1.4426950408889634
NEG_FILL = -1e30
NORM_EPS = 1e-06
MESH = pl.DeviceIdType.MESH


def norm_rows(values_in, gain_vec):
    widened = values_in.astype(jnp.float32)
    return (
        widened
        * lax.rsqrt(jnp.mean(widened * widened, axis=-1, keepdims=True) + NORM_EPS)
        * gain_vec
    )


def three_pieces(wide):
    high = wide.astype(jnp.bfloat16)
    rest = wide - high.astype(jnp.float32)
    middle = rest.astype(jnp.bfloat16)
    low = (rest - middle.astype(jnp.float32)).astype(jnp.bfloat16)
    return high, middle, low


def contract(a, b, left, right):
    return lax.dot_general(
        a, b, (((left,), (right,)), ((), ())), preferred_element_type=jnp.float32
    )


def flip(place, step, size):
    total = 0
    bit = 1
    while bit < size:
        total = total + lax.rem(place // bit + step // bit, 2) * bit
        bit *= 2
    return total


def fused_kernel(
    n_ep, x_hbm, gate_ref, gain_ref, wq_hbm, wk_hbm, wv_hbm, wo_hbm, post_ref, xin_hbm,
    ids_ref, share_ref, egain_ref, wg_hbm, wu_hbm, wd_hbm, epost_ref,
    mixer_ref, expert_ref,
    x_v, wq_v, wkv_v, wo_v, xin_v, wgu_v, wd_v, out_rows, slots, product, arrived, summed,
    crossed, final, returned, weigh_v, kv_all, q_full, max_ref, acc_ref, mixed_v, heads_v,
    l_sem, ep_sem, x_sem, c_sem, d_sem, p_sem, r_sem, s_sem, b_sem, k_sem, f_sem, h_sem,
):
    own = lax.axis_index("ep")
    quarter = lax.axis_index("tp")
    across = lax.rem(quarter + 2, 4)
    beside = quarter + 1 - 2 * lax.rem(quarter, 2)
    diagonal = lax.rem(beside + 2, 4)
    column = lax.rem(own, 2)
    row = own // 2
    row_total = n_ep // 2
    partner = own + 1 - 2 * column
    heads, _, rows = q_full.shape
    token_rows = xin_v.shape[0]
    cap = out_rows.shape[1]
    width = out_rows.shape[2]
    units = wd_v.shape[0]

    def remote(source, target, sems, at_send, at_recv, axis, place):
        return pltpu.make_async_remote_copy(
            src_ref=source, dst_ref=target, send_sem=sems.at[0, at_send],
            recv_sem=sems.at[1, at_recv], device_id={axis: place}, device_id_type=MESH,
        )

    def local(index):
        pairs = (
            (xin_hbm.at[pl.ds(quarter * token_rows, token_rows)], xin_v),
            (x_hbm, x_v),
            (wk_hbm, wkv_v.at[0:HD]),
            (wv_hbm, wkv_v.at[HD : 2 * HD]),
            (wq_hbm, wq_v),
            (wg_hbm, wgu_v.at[:, 0:units]),
            (wu_hbm, wgu_v.at[:, units : 2 * units]),
            (wd_hbm, wd_v),
            (wo_hbm, wo_v),
        )
        return pltpu.make_async_copy(pairs[index][0], pairs[index][1], l_sem.at[index])

    for index in range(9):
        local(index).start()
    barrier = pltpu.get_barrier_semaphore()
    for axis, size in (("ep", n_ep), ("tp", 4)):
        place = lax.axis_index(axis)
        for step in range(1, size):
            pl.semaphore_signal(
                barrier, inc=1, device_id={axis: lax.rem(place + step, size)},
                device_id_type=MESH,
            )

    def ep_copy(source, place):
        return remote(
            out_rows.at[place], slots.at[quarter, source], ep_sem, place, source, "ep", place
        )

    def to_across(source):
        held = slots.at[quarter, source]
        return remote(held, held, x_sem, source, source, "tp", across)

    def from_across(source):
        held = slots.at[across, source]
        return remote(held, held, x_sem, source, source, "tp", across)

    def to_beside(source):
        held = slots.at[quarter, source]
        return remote(held, held, c_sem, source, source, "tp", beside)

    def from_beside(source):
        held = slots.at[beside, source]
        return remote(held, held, c_sem, source, source, "tp", beside)

    def second(source):
        held = slots.at[across, source]
        return remote(held, held, d_sem, source, source, "tp", beside)

    def from_second(source):
        held = slots.at[diagonal, source]
        return remote(held, held, d_sem, source, source, "tp", beside)

    def near(j):
        return remote(product.at[beside, j], arrived.at[0, j], p_sem, j, j, "tp", beside)

    def far(j):
        return remote(product.at[diagonal, j], arrived.at[1, j], r_sem, j, j, "tp", beside)

    def cross(j):
        return remote(summed.at[j], crossed.at[j], s_sem, j, j, "tp", across)

    def home(j, source):
        return remote(final.at[j], returned.at[source], b_sem, j, source, "ep", j)

    def chain(source, place):
        return remote(kv_all.at[source], kv_all.at[source], k_sem, source, source, "ep", place)

    def hand(source):
        return remote(kv_all.at[source], kv_all.at[source], f_sem, source, source, "ep", partner)

    def heads_copy(step):
        place = lax.rem(quarter + step, 4)
        return remote(mixed_v.at[place], heads_v.at[quarter], h_sem, step, step, "tp", place)

    def own_part(wide):
        part = 0
        for k in range(4):
            chosen = (quarter == k).astype(wide.dtype)
            part = part + wide[:, k * token_rows : (k + 1) * token_rows] * chosen
        return part

    ids = own_part(ids_ref[...])
    shares = own_part(share_ref[...])
    expert = lax.broadcasted_iota(jnp.int32, (n_ep, token_rows), 0)
    first_is = (expert == ids[0:1]).astype(jnp.float32)
    second_is = (expert == ids[1:2]).astype(jnp.float32)
    named = (first_is + second_is).astype(jnp.bfloat16)
    earlier = (
        lax.broadcasted_iota(jnp.int32, (token_rows, token_rows), 0)
        < lax.broadcasted_iota(jnp.int32, (token_rows, token_rows), 1)
    ).astype(jnp.bfloat16)
    before = jnp.dot(named, earlier, preferred_element_type=jnp.float32).astype(jnp.bfloat16)
    total = n_ep * cap
    at_row = lax.broadcasted_iota(jnp.int32, (total, n_ep), 0)
    low_row = lax.broadcasted_iota(jnp.int32, (total, n_ep), 1) * cap
    spread = ((at_row >= low_row) & (at_row < low_row + cap)).astype(jnp.bfloat16)
    rank = (lax.broadcasted_iota(jnp.int32, (total, token_rows), 0) & (cap - 1)).astype(
        jnp.float32
    )
    here = jnp.dot(spread, before, preferred_element_type=jnp.float32) == rank
    sel = jnp.where(here, jnp.dot(spread, named, preferred_element_type=jnp.float32), 0.0)
    local(0).wait()
    normed_m = norm_rows(xin_v[...], egain_ref[...]).astype(jnp.bfloat16)
    outgoing = jnp.dot(sel.astype(jnp.bfloat16), normed_m, preferred_element_type=jnp.float32)
    out_rows[...] = outgoing.astype(jnp.bfloat16).reshape(out_rows.shape)
    slots[quarter, own] = out_rows[own]
    pl.semaphore_wait(barrier, n_ep - 1 + 3)
    for step in range(1, 4):
        ep_copy(own, flip(own, step, n_ep)).start()
    to_across(own).start()
    to_beside(own).start()

    local(1).wait()
    slab = min(64, rows)

    def norm_slab(index, carry):
        at = pl.ds(pl.multiple_of(index * slab, slab), slab)
        x_v[at] = norm_rows(x_v[at], gain_ref[...]).astype(jnp.bfloat16)
        return carry

    lax.fori_loop(0, rows // slab, norm_slab, 0)
    local(2).wait()
    local(3).wait()
    kv_all[own] = contract(x_v[...], wkv_v[...], 1, 1).astype(jnp.bfloat16)

    @pl.when(row + 1 < row_total)
    def _():
        chain(own, own + 2).start()

    @pl.when(column == 0)
    def _():
        hand(own).start()

    local(4).wait()
    queries = jnp.dot(x_v[...], wq_v[...], preferred_element_type=jnp.float32)
    queries = queries.astype(jnp.bfloat16).astype(jnp.float32).T * (LOG2E * HD ** (-0.5))
    piece_row = lax.broadcasted_iota(jnp.int32, (HD, rows), 0)
    for head in range(heads):
        wide = queries[head * HD : (head + 1) * HD]
        high = wide.astype(jnp.bfloat16)
        q_full[head, 0:HD] = high
        q_full[head, HD : 2 * HD] = jnp.zeros((HD, rows), jnp.bfloat16)
        q_full[head, 2 * HD : 3 * HD] = (wide - high.astype(jnp.float32)).astype(jnp.bfloat16)
        ones = (piece_row == head) | (piece_row == heads + head) | (piece_row == 2 * heads + head)
        q_full[head, 3 * HD : 4 * HD] = ones.astype(jnp.bfloat16)

    low_lane = lax.broadcasted_iota(jnp.int32, (n_ep, total), 0) * cap
    at_lane = lax.broadcasted_iota(jnp.int32, (n_ep, total), 1)
    spread_t = ((at_lane >= low_lane) & (at_lane < low_lane + cap)).astype(jnp.bfloat16)
    rank_t = (lax.broadcasted_iota(jnp.int32, (token_rows, total), 1) & (cap - 1)).astype(
        jnp.float32
    )
    here_t = contract(before, spread_t, 0, 0) == rank_t
    weighed = first_is * shares[0:1] + second_is * shares[1:2]
    for index, piece in enumerate(three_pieces(weighed)):
        placed = jnp.where(here_t, contract(piece, spread_t, 0, 0), 0.0)
        weigh_v[index * token_rows : (index + 1) * token_rows] = placed.astype(jnp.bfloat16)

    max_ref[...] = jnp.full(max_ref.shape, NEG_FILL, jnp.float32)
    acc_ref[...] = jnp.zeros(acc_ref.shape, jnp.float32)

    def attend(index, diag):
        kv = kv_all[index]
        first = pl.multiple_of(index * rows, rows)
        pieces = three_pieces(gate_ref[:, pl.ds(first, rows)] * (-LOG2E))
        pieces = [piece.astype(jnp.float32) for piece in pieces]
        stacked = jnp.concatenate(
            [jnp.zeros((HD, rows), jnp.float32)]
            + pieces
            + [jnp.zeros((HD - 3 * heads, rows), jnp.float32)],
            axis=0,
        )
        lane = lax.broadcasted_iota(jnp.int32, kv.shape, 1)
        gated = jnp.where(lane < HD, kv, stacked.T.astype(jnp.bfloat16))
        keys = jnp.concatenate([kv, gated], axis=1)
        values = kv.T
        at = lax.broadcasted_iota(jnp.int32, values.shape, 0)
        values = jnp.where(at < HD, jnp.ones_like(values), values)[HD - ONES :]
        for head in range(heads):
            scores = jnp.dot(keys, q_full[head], preferred_element_type=jnp.float32)
            if diag:
                key = lax.broadcasted_iota(jnp.int32, scores.shape, 0)
                query = lax.broadcasted_iota(jnp.int32, scores.shape, 1)
                scores = jnp.where(key <= query, scores, NEG_FILL)
            old_max = max_ref[head]
            new_max = jnp.maximum(old_max, jnp.max(scores, axis=0, keepdims=True))
            shifted = jnp.exp2(scores - new_max).astype(jnp.bfloat16)
            acc_ref[head] = acc_ref[head] * jnp.exp2(old_max - new_max) + jnp.dot(
                values, shifted, preferred_element_type=jnp.float32
            )
            max_ref[head] = new_max

    attend(own, True)
    for index in (5, 6, 7):
        local(index).wait()

    def block_of(t):
        return own + lax.rem(t, 2) * (partner - own) - 2 * (t // 2)

    def run(t, carry):
        @pl.when(t + 4 < n_ep)
        def _():
            ep_copy(own, flip(own, t + 4, n_ep)).start()

        @pl.when((t > 0) & (t < n_ep))
        def _():
            source = flip(own, t, n_ep)
            ep_copy(source, source).wait_recv()
            to_across(source).start()
            to_beside(source).start()

        @pl.when((t > 0) & (lax.rem(t, 2) == 0) & (t // 2 <= row))
        def _():
            source = own - t
            chain(source, own).wait_recv()
            hand(source).start()

            @pl.when(row + 1 < row_total)
            def _():
                chain(source, own + 2).start()

        @pl.when((t >= 1) & (t <= n_ep))
        def _():
            source = flip(own, t - 1, n_ep)
            from_across(source).wait_recv()
            second(source).start()

        @pl.when(t >= 4)
        def _():
            j = flip(own, t - 4, n_ep)
            near(j).wait_recv()
            cross(j).wait_recv()
            whole = product[quarter, j].astype(jnp.float32) + arrived[0, j].astype(jnp.float32)
            final[j] = (whole + crossed[j].astype(jnp.float32)).astype(jnp.bfloat16)

            @pl.when(t > 4)
            def _():
                home(j, own).start()

        @pl.when((t >= 3) & (t < n_ep + 3))
        def _():
            j = flip(own, t - 3, n_ep)
            far(j).wait_recv()
            pair = product[across, j].astype(jnp.float32) + arrived[1, j].astype(jnp.float32)
            summed[j] = pair.astype(jnp.bfloat16)
            cross(j).start()

        @pl.when((t >= 2) & (t < n_ep + 2))
        def _():
            source = flip(own, t - 2, n_ep)
            from_beside(source).wait_recv()
            from_second(source).wait_recv()
            tokens = slots[:, source].reshape(4 * cap, width)
            both = jnp.dot(tokens, wgu_v[...], preferred_element_type=jnp.float32)
            gate_part = both[:, :units]
            hidden = gate_part / (1.0 + jnp.exp(-gate_part)) * both[:, units:]
            terms = jnp.dot(
                hidden.astype(jnp.bfloat16), wd_v[...], preferred_element_type=jnp.float32
            )
            product[:, source] = terms.astype(jnp.bfloat16).reshape(4, cap, width)
            far(source).start()
            near(source).start()

        @pl.when((t >= 2) & (t <= n_ep))
        def _():
            turn = t - 1

            @pl.when((turn // 2 <= row) & ((turn > 1) | (column == 1)))
            def _():
                block = block_of(turn)

                @pl.when(lax.rem(turn, 2) == 1)
                def _():
                    hand(block).wait_recv()

                attend(block, False)

        @pl.when(t == n_ep + 1)
        def _():
            parts = [acc_ref[head, ONES:] / acc_ref[head, 0:1] for head in range(heads)]
            mixed = jnp.concatenate(parts, axis=0).T.astype(jnp.bfloat16)
            mixed_v[...] = mixed.reshape(mixed_v.shape)
            for step in range(1, 4):
                heads_copy(step).start()
            heads_v[quarter] = mixed_v[quarter]

        return carry

    lax.fori_loop(0, n_ep + 4, run, 0)
    returned[own] = final[own]

    for step in range(1, 4):
        heads_copy(step).wait()
    local(8).wait()
    by_rows = jnp.concatenate([heads_v[k] for k in range(4)], axis=1)
    projected = jnp.dot(by_rows, wo_v[...], preferred_element_type=jnp.float32)
    mixer_ref[...] = norm_rows(projected, post_ref[...]).astype(jnp.bfloat16)

    def come_home(step, carry):
        j = flip(own, step, n_ep)
        home(j, j).wait_recv()
        return carry

    lax.fori_loop(1, n_ep, come_home, 0)
    rows_back = returned[...].reshape(total, width)
    picked = jnp.dot(weigh_v[...], rows_back, preferred_element_type=jnp.float32)
    combined = picked[:token_rows] + picked[token_rows : 2 * token_rows]
    combined = combined + picked[2 * token_rows :]
    expert_ref[...] = norm_rows(combined, epost_ref[...]).astype(jnp.bfloat16)

    def drain(step, carry):
        j = flip(own, step, n_ep)
        to_across(j).wait_send()
        to_beside(j).wait_send()
        second(j).wait_send()
        near(j).wait_send()
        far(j).wait_send()
        cross(j).wait_send()

        @pl.when(step > 0)
        def _():
            ep_copy(own, j).wait_send()
            home(j, own).wait_send()

        return carry

    lax.fori_loop(0, n_ep, drain, 0)

    def drain_kv(step, carry):
        source = own - 2 * step

        @pl.when((step <= row) & (row + 1 < row_total))
        def _():
            chain(source, own + 2).wait_send()

        @pl.when((step <= row) & ((step > 0) | (column == 0)))
        def _():
            hand(source).wait_send()

        return carry

    lax.fori_loop(0, row_total, drain_kv, 0)


def per_device(
    mixer_input, log_forget_total, mixer_gain, w_query, w_key, w_value, w_output,
    mixer_post_gain, expert_input, expert_ids, route_weight, expert_gain, w_gate, w_up,
    w_down, expert_post_gain,
):
    n_ep = lax.axis_size("ep")
    rows, width = mixer_input.shape
    head_columns = w_query.shape[1]
    heads = head_columns // HD
    token_rows = expert_input.shape[0] // 4
    cap = 2 * TOP_K * token_rows // n_ep
    units = w_gate.shape[2]
    out_columns = w_output.shape[0]
    half = jnp.bfloat16
    chunk = (n_ep, cap, width)
    pair = pltpu.SemaphoreType.DMA((2, n_ep))
    vmem = pl.BlockSpec(memory_space=pltpu.VMEM)
    anywhere = pl.BlockSpec(memory_space=pl.ANY)
    scratch = [
        pltpu.VMEM((rows, width), half),
        pltpu.VMEM((width, head_columns), half),
        pltpu.VMEM((2 * HD, width), half),
        pltpu.VMEM((out_columns, width), half),
        pltpu.VMEM((token_rows, width), half),
        pltpu.VMEM((width, 2 * units), half),
        pltpu.VMEM((units, width), half),
        pltpu.VMEM(chunk, half),
        pltpu.VMEM((4,) + chunk, half),
        pltpu.VMEM((4,) + chunk, half),
        pltpu.VMEM((2,) + chunk, half),
        pltpu.VMEM(chunk, half),
        pltpu.VMEM(chunk, half),
        pltpu.VMEM(chunk, half),
        pltpu.VMEM(chunk, half),
        pltpu.VMEM((3 * token_rows, n_ep * cap), half),
        pltpu.VMEM((n_ep, rows, 2 * HD), half),
        pltpu.VMEM((heads, 4 * HD, rows), half),
        pltpu.VMEM((heads, 1, rows), jnp.float32),
        pltpu.VMEM((heads, HD + ONES, rows), jnp.float32),
        pltpu.VMEM((4, rows // 4, head_columns), half),
        pltpu.VMEM((4, rows // 4, head_columns), half),
        pltpu.SemaphoreType.DMA((9,)),
    ] + [pair] * 10 + [pltpu.SemaphoreType.DMA((2, 4))]
    return pl.pallas_call(
        functools.partial(fused_kernel, n_ep),
        out_shape=(
            jax.ShapeDtypeStruct((rows // 4, width), half),
            jax.ShapeDtypeStruct((token_rows, width), half),
        ),
        in_specs=[
            anywhere, vmem, vmem, anywhere, anywhere, anywhere, anywhere, vmem, anywhere,
            vmem, vmem, vmem, anywhere, anywhere, anywhere, vmem,
        ],
        out_specs=(vmem, vmem),
        scratch_shapes=scratch,
        compiler_params=pltpu.CompilerParams(
            collective_id=0, has_side_effects=True, vmem_limit_bytes=60 * 1024 * 1024
        ),
        name="fused",
    )(
        mixer_input, log_forget_total, mixer_gain[None], w_query, w_key.T, w_value.T, w_output,
        mixer_post_gain[None], expert_input, expert_ids.T, route_weight.T, expert_gain[None],
        w_gate[0], w_up[0], w_down[0], expert_post_gain[None],
    )


def solution(mesh):
    placed = (
        P("ep", None),
        P("tp", None),
        P(),
        P(None, "tp"),
        P(None, "tp"),
        P(None, "tp"),
        P(),
        P(),
        P("ep", None),
        P("ep", None),
        P("ep", None),
        P(),
        P("ep", None, "tp"),
        P("ep", None, "tp"),
        P("ep", "tp", None),
        P(),
    )
    return jax.shard_map(
        per_device,
        mesh=mesh,
        in_specs=placed,
        out_specs=(P(("ep", "tp"), None), P(("ep", "tp"), None)),
        check_vma=False,
    )
```

time: 138 us -> 84 us (0.61)
  the two profiles are of different devices: /device:TPU:17 before, /device:TPU:12 now
where the time goes in v1:
time: 84 us; the launch traced here: 83.7 us
  Pallas kernels  79.5 us (95%)
  local copies, waits for them, and re-layouts  3.55 us (4%)
    pallas_call x1, Pallas kernels, per_device(): pl.pallas_call(functools.partial(fused_kernel, n_ep), out_shape=(jax.Shap...  79.5 us
    unnamed x2, local copies, waits for them, and re-layouts  3.55 us

profile of v1, /device:TPU:12, one launch (start us, length us, event | category | flops | bytes accessed | tf_op | source)
XLA Modules:
  0.0 83.7 jit_solution(11011627925033087876)
XLA Ops:
  0.6 79.5 %fused.1 = (bf16[128,2048]{1,0:T(8,128)(2,1)}, bf16[64,2048]{1,0:T(8,128)(2,1)}) custom-call(bf16[512,2048]{1,0:T(8,128)(2,1)} %x_hbm.1, f32[4,4096]{1,0:T(4,128)} %gate_ref.1, f32[1,2048]{1,0:T(1,128)} %bitcast.16, bf16[2048,256]{1,0:T(8,128)(2,1)} %wq_hbm.1, bf16[64,2048]{1,0:T(8,128)(2,1)} %bitcast.14, bf16[64,2048]{1,0:T(8,128)(2,1)} %bitcast.15, ...), custom_call_target="tpu_custom_call" | custom-call | tf_op jit(solution)/shard_map/fused/pallas_call | solution.py:469
  80.2 1.9 %copy.20 = bf16[128,2048]{1,0:T(8,128)(2,1)} copy(bf16[128,2048]{1,0:T(8,128)(2,1)} %get-tuple-element.4) | data formatting | bytes 1048576
  82.0 1.7 %copy.21 = bf16[64,2048]{1,0:T(8,128)(2,1)} copy(bf16[64,2048]{1,0:T(8,128)(2,1)} %get-tuple-element.5) | data formatting | bytes 524288

commit v2 on v1

--- a/solution.py
+++ b/solution.py
@@ -14,6 +14,8 @@
 NEG_FILL = -1e30
 NORM_EPS = 1e-06
 MESH = pl.DeviceIdType.MESH
+SOON = 5
+LATER = 8
 
 
 def norm_rows(values_in, gain_vec):
@@ -49,10 +51,10 @@
 
 
 def fused_kernel(
-    n_ep, x_hbm, gate_ref, gain_ref, wq_hbm, wk_hbm, wv_hbm, wo_hbm, post_ref, xin_hbm,
-    ids_ref, share_ref, egain_ref, wg_hbm, wu_hbm, wd_hbm, epost_ref,
+    n_ep, x_hbm, gate_hbm, gain_hbm, wq_hbm, wk_hbm, wv_hbm, wo_hbm, post_hbm, xin_hbm,
+    ids_hbm, share_hbm, egain_hbm, wg_hbm, wu_hbm, wd_hbm, epost_hbm,
     mixer_ref, expert_ref,
-    x_v, wq_v, wkv_v, wo_v, xin_v, wgu_v, wd_v, out_rows, slots, product, arrived, summed,
+    gate_ref, gain_ref, post_ref, ids_ref, share_ref, egain_ref, epost_ref, x_v, wq_v, wkv_v, wo_v, xin_v, wgu_v, wd_v, out_rows, slots, product, arrived, summed,
     crossed, final, returned, weigh_v, kv_all, q_full, max_ref, acc_ref, mixed_v, heads_v,
     l_sem, ep_sem, x_sem, c_sem, d_sem, p_sem, r_sem, s_sem, b_sem, k_sem, f_sem, h_sem,
 ):
@@ -79,19 +81,26 @@
 
     def local(index):
         pairs = (
+            (ids_hbm, ids_ref),
             (xin_hbm.at[pl.ds(quarter * token_rows, token_rows)], xin_v),
+            (egain_hbm, egain_ref),
+            (share_hbm, share_ref),
             (x_hbm, x_v),
+            (gain_hbm, gain_ref),
             (wk_hbm, wkv_v.at[0:HD]),
             (wv_hbm, wkv_v.at[HD : 2 * HD]),
             (wq_hbm, wq_v),
+            (gate_hbm, gate_ref),
             (wg_hbm, wgu_v.at[:, 0:units]),
             (wu_hbm, wgu_v.at[:, units : 2 * units]),
             (wd_hbm, wd_v),
             (wo_hbm, wo_v),
+            (post_hbm, post_ref),
+            (epost_hbm, epost_ref),
         )
         return pltpu.make_async_copy(pairs[index][0], pairs[index][1], l_sem.at[index])
 
-    for index in range(9):
+    for index in range(16):
         local(index).start()
     barrier = pltpu.get_barrier_semaphore()
     for axis, size in (("ep", n_ep), ("tp", 4)):
@@ -153,6 +162,9 @@
         place = lax.rem(quarter + step, 4)
         return remote(mixed_v.at[place], heads_v.at[quarter], h_sem, step, step, "tp", place)
 
+    def peer(step):
+        return flip(own, step, n_ep)
+
     def own_part(wide):
         part = 0
         for k in range(4):
@@ -160,8 +172,8 @@
             part = part + wide[:, k * token_rows : (k + 1) * token_rows] * chosen
         return part
 
+    local(0).wait()
     ids = own_part(ids_ref[...])
-    shares = own_part(share_ref[...])
     expert = lax.broadcasted_iota(jnp.int32, (n_ep, token_rows), 0)
     first_is = (expert == ids[0:1]).astype(jnp.float32)
     second_is = (expert == ids[1:2]).astype(jnp.float32)
@@ -180,18 +192,20 @@
     )
     here = jnp.dot(spread, before, preferred_element_type=jnp.float32) == rank
     sel = jnp.where(here, jnp.dot(spread, named, preferred_element_type=jnp.float32), 0.0)
-    local(0).wait()
+    local(1).wait()
+    local(2).wait()
     normed_m = norm_rows(xin_v[...], egain_ref[...]).astype(jnp.bfloat16)
     outgoing = jnp.dot(sel.astype(jnp.bfloat16), normed_m, preferred_element_type=jnp.float32)
     out_rows[...] = outgoing.astype(jnp.bfloat16).reshape(out_rows.shape)
     slots[quarter, own] = out_rows[own]
     pl.semaphore_wait(barrier, n_ep - 1 + 3)
-    for step in range(1, 4):
-        ep_copy(own, flip(own, step, n_ep)).start()
+    for step in range(1, SOON):
+        ep_copy(own, peer(step)).start()
     to_across(own).start()
     to_beside(own).start()
 
-    local(1).wait()
+    local(4).wait()
+    local(5).wait()
     slab = min(64, rows)
 
     def norm_slab(index, carry):
@@ -200,8 +214,8 @@
         return carry
 
     lax.fori_loop(0, rows // slab, norm_slab, 0)
-    local(2).wait()
-    local(3).wait()
+    local(6).wait()
+    local(7).wait()
     kv_all[own] = contract(x_v[...], wkv_v[...], 1, 1).astype(jnp.bfloat16)
 
     @pl.when(row + 1 < row_total)
@@ -212,7 +226,12 @@
     def _():
         hand(own).start()
 
-    local(4).wait()
+    def send_rest(step, carry):
+        ep_copy(own, peer(step)).start()
+        return carry
+
+    lax.fori_loop(SOON, n_ep, send_rest, 0)
+    local(8).wait()
     queries = jnp.dot(x_v[...], wq_v[...], preferred_element_type=jnp.float32)
     queries = queries.astype(jnp.bfloat16).astype(jnp.float32).T * (LOG2E * HD ** (-0.5))
     piece_row = lax.broadcasted_iota(jnp.int32, (HD, rows), 0)
@@ -232,6 +251,8 @@
         jnp.float32
     )
     here_t = contract(before, spread_t, 0, 0) == rank_t
+    local(3).wait()
+    shares = own_part(share_ref[...])
     weighed = first_is * shares[0:1] + second_is * shares[1:2]
     for index, piece in enumerate(three_pieces(weighed)):
         placed = jnp.where(here_t, contract(piece, spread_t, 0, 0), 0.0)
@@ -271,28 +292,60 @@
             )
             max_ref[head] = new_max
 
-    attend(own, True)
-    for index in (5, 6, 7):
+    for index in (9, 10, 11, 12):
         local(index).wait()
 
     def block_of(t):
         return own + lax.rem(t, 2) * (partner - own) - 2 * (t // 2)
 
+    def pass_across(step):
+        j = peer(step)
+        far(j).wait_recv()
+        pair = product[across, j].astype(jnp.float32) + arrived[1, j].astype(jnp.float32)
+        summed[j] = pair.astype(jnp.bfloat16)
+        cross(j).start()
+
+    def finish(step):
+        j = peer(step)
+        near(j).wait_recv()
+        cross(j).wait_recv()
+        whole = product[quarter, j].astype(jnp.float32) + arrived[0, j].astype(jnp.float32)
+        final[j] = (whole + crossed[j].astype(jnp.float32)).astype(jnp.bfloat16)
+
+        @pl.when(step > 0)
+        def _():
+            home(j, own).start()
+
+    half = n_ep // 2
+
+    def by_urgency(step, task):
+        @pl.when((step >= half) & (step < n_ep))
+        def _():
+            task(step)
+
+        near_step = step - half + 1 - 0
+
+        @pl.when((near_step >= 1) & (near_step < half))
+        def _():
+            task(near_step)
+
+        @pl.when(step == n_ep)
+        def _():
+            task(0)
+
     def run(t, carry):
-        @pl.when(t + 4 < n_ep)
-        def _():
-            ep_copy(own, flip(own, t + 4, n_ep)).start()
-
         @pl.when((t > 0) & (t < n_ep))
         def _():
-            source = flip(own, t, n_ep)
+            source = peer(t)
             ep_copy(source, source).wait_recv()
             to_across(source).start()
             to_beside(source).start()
 
-        @pl.when((t > 0) & (lax.rem(t, 2) == 0) & (t // 2 <= row))
-        def _():
-            source = own - t
+        early = t - LATER + 2
+
+        @pl.when((early > 0) & (lax.rem(early + n_ep, 2) == 0) & (early <= 2 * row))
+        def _():
+            source = own - early
             chain(source, own).wait_recv()
             hand(source).start()
 
@@ -300,35 +353,17 @@
             def _():
                 chain(source, own + 2).start()
 
-        @pl.when((t >= 1) & (t <= n_ep))
-        def _():
-            source = flip(own, t - 1, n_ep)
+        @pl.when((t >= 2) & (t < n_ep + 2))
+        def _():
+            source = peer(t - 2)
             from_across(source).wait_recv()
             second(source).start()
 
-        @pl.when(t >= 4)
-        def _():
-            j = flip(own, t - 4, n_ep)
-            near(j).wait_recv()
-            cross(j).wait_recv()
-            whole = product[quarter, j].astype(jnp.float32) + arrived[0, j].astype(jnp.float32)
-            final[j] = (whole + crossed[j].astype(jnp.float32)).astype(jnp.bfloat16)
-
-            @pl.when(t > 4)
-            def _():
-                home(j, own).start()
+        by_urgency(t - 4, pass_across)
 
         @pl.when((t >= 3) & (t < n_ep + 3))
         def _():
-            j = flip(own, t - 3, n_ep)
-            far(j).wait_recv()
-            pair = product[across, j].astype(jnp.float32) + arrived[1, j].astype(jnp.float32)
-            summed[j] = pair.astype(jnp.bfloat16)
-            cross(j).start()
-
-        @pl.when((t >= 2) & (t < n_ep + 2))
-        def _():
-            source = flip(own, t - 2, n_ep)
+            source = peer(t - 3)
             from_beside(source).wait_recv()
             from_second(source).wait_recv()
             tokens = slots[:, source].reshape(4 * cap, width)
@@ -342,9 +377,13 @@
             far(source).start()
             near(source).start()
 
-        @pl.when((t >= 2) & (t <= n_ep))
-        def _():
-            turn = t - 1
+        @pl.when(t == 2)
+        def _():
+            attend(own, True)
+
+        @pl.when((t > LATER) & (t < n_ep + LATER))
+        def _():
+            turn = t - LATER
 
             @pl.when((turn // 2 <= row) & ((turn > 1) | (column == 1)))
             def _():
@@ -356,7 +395,11 @@
 
                 attend(block, False)
 
-        @pl.when(t == n_ep + 1)
+        by_urgency(t - 5, finish)
+
+        done = t - LATER - 2 * row
+
+        @pl.when(done == 1)
         def _():
             parts = [acc_ref[head, ONES:] / acc_ref[head, 0:1] for head in range(heads)]
             mixed = jnp.concatenate(parts, axis=0).T.astype(jnp.bfloat16)
@@ -365,17 +408,20 @@
                 heads_copy(step).start()
             heads_v[quarter] = mixed_v[quarter]
 
+        @pl.when(t == n_ep + LATER)
+        def _():
+            for step in range(1, 4):
+                heads_copy(step).wait()
+            local(13).wait()
+            local(14).wait()
+            by_rows = jnp.concatenate([heads_v[k] for k in range(4)], axis=1)
+            projected = jnp.dot(by_rows, wo_v[...], preferred_element_type=jnp.float32)
+            mixer_ref[...] = norm_rows(projected, post_ref[...]).astype(jnp.bfloat16)
+
         return carry
 
-    lax.fori_loop(0, n_ep + 4, run, 0)
+    lax.fori_loop(0, n_ep + max(LATER + 1, 5 + 1), run, 0)
     returned[own] = final[own]
-
-    for step in range(1, 4):
-        heads_copy(step).wait()
-    local(8).wait()
-    by_rows = jnp.concatenate([heads_v[k] for k in range(4)], axis=1)
-    projected = jnp.dot(by_rows, wo_v[...], preferred_element_type=jnp.float32)
-    mixer_ref[...] = norm_rows(projected, post_ref[...]).astype(jnp.bfloat16)
 
     def come_home(step, carry):
         j = flip(own, step, n_ep)
@@ -383,6 +429,7 @@
         return carry
 
     lax.fori_loop(1, n_ep, come_home, 0)
+    local(15).wait()
     rows_back = returned[...].reshape(total, width)
     picked = jnp.dot(weigh_v[...], rows_back, preferred_element_type=jnp.float32)
     combined = picked[:token_rows] + picked[token_rows : 2 * token_rows]
@@ -440,8 +487,16 @@
     chunk = (n_ep, cap, width)
     pair = pltpu.SemaphoreType.DMA((2, n_ep))
     vmem = pl.BlockSpec(memory_space=pltpu.VMEM)
-    anywhere = pl.BlockSpec(memory_space=pl.ANY)
+    far_memory = pl.BlockSpec(memory_space=pltpu.HBM)
+    gains = pltpu.VMEM((1, width), jnp.float32)
     scratch = [
+        pltpu.VMEM(log_forget_total.shape, jnp.float32),
+        gains,
+        gains,
+        pltpu.VMEM((TOP_K, 4 * token_rows), jnp.int32),
+        pltpu.VMEM((TOP_K, 4 * token_rows), jnp.float32),
+        gains,
+        gains,
         pltpu.VMEM((rows, width), half),
         pltpu.VMEM((width, head_columns), half),
         pltpu.VMEM((2 * HD, width), half),
@@ -464,7 +519,7 @@
         pltpu.VMEM((heads, HD + ONES, rows), jnp.float32),
         pltpu.VMEM((4, rows // 4, head_columns), half),
         pltpu.VMEM((4, rows // 4, head_columns), half),
-        pltpu.SemaphoreType.DMA((9,)),
+        pltpu.SemaphoreType.DMA((16,)),
     ] + [pair] * 10 + [pltpu.SemaphoreType.DMA((2, 4))]
     return pl.pallas_call(
         functools.partial(fused_kernel, n_ep),
@@ -472,10 +527,7 @@
             jax.ShapeDtypeStruct((rows // 4, width), half),
             jax.ShapeDtypeStruct((token_rows, width), half),
         ),
-        in_specs=[
-            anywhere, vmem, vmem, anywhere, anywhere, anywhere, anywhere, vmem, anywhere,
-            vmem, vmem, vmem, anywhere, anywhere, anywhere, vmem,
-        ],
+        in_specs=[far_memory] * 16,
         out_specs=(vmem, vmem),
         scratch_shapes=scratch,
         compiler_params=pltpu.CompilerParams(

time: 84 us -> 71.2 us (0.85)
  the two profiles are of different devices: /device:TPU:12 before, /device:TPU:17 now
where the time goes in v2:
time: 71.2 us; the launch traced here: 71 us
  Pallas kernels  66.8 us (94%)
  local copies, waits for them, and re-layouts  3.55 us (5%)
    pallas_call x1, Pallas kernels, per_device(): pl.pallas_call(functools.partial(fused_kernel, n_ep), out_shape=(jax.Shap...  66.8 us
    unnamed x2, local copies, waits for them, and re-layouts  3.55 us

profile of v2, /device:TPU:17, one launch (start us, length us, event | category | flops | bytes accessed | tf_op | source)
XLA Modules:
  0.0 71.0 jit_solution(12450519419350789444)
XLA Ops:
  0.6 66.8 %fused.1 = (bf16[128,2048]{1,0:T(8,128)(2,1)}, bf16[64,2048]{1,0:T(8,128)(2,1)}) custom-call(bf16[512,2048]{1,0:T(8,128)(2,1)} %x_hbm.1, f32[4,4096]{1,0:T(4,128)} %gate_hbm.1, f32[1,2048]{1,0:T(1,128)} %bitcast.16, bf16[2048,256]{1,0:T(8,128)(2,1)} %wq_hbm.1, bf16[64,2048]{1,0:T(8,128)(2,1)} %bitcast.14, bf16[64,2048]{1,0:T(8,128)(2,1)} %bitcast.15, ...), custom_call_target="tpu_custom_call" | custom-call | tf_op jit(solution)/shard_map/fused/pallas_call | solution.py:524
  67.5 1.9 %copy.20 = bf16[128,2048]{1,0:T(8,128)(2,1)} copy(bf16[128,2048]{1,0:T(8,128)(2,1)} %get-tuple-element.4) | data formatting | bytes 1048576
  69.4 1.7 %copy.21 = bf16[64,2048]{1,0:T(8,128)(2,1)} copy(bf16[64,2048]{1,0:T(8,128)(2,1)} %get-tuple-element.5) | data formatting | bytes 524288

commit v3 on v2

--- a/solution.py
+++ b/solution.py
@@ -318,20 +318,35 @@
 
     half = n_ep // 2
 
-    def by_urgency(step, task):
+    def cross_over(step):
+        near_step = step - half + 1
+
         @pl.when((step >= half) & (step < n_ep))
         def _():
-            task(step)
-
-        near_step = step - half + 1 - 0
+            pass_across(step)
 
         @pl.when((near_step >= 1) & (near_step < half))
         def _():
-            task(near_step)
+            pass_across(near_step)
 
         @pl.when(step == n_ep)
         def _():
-            task(0)
+            pass_across(0)
+
+    def send_home(step):
+        near_step = step - half + 1
+
+        @pl.when((step >= half) & (step < n_ep))
+        def _():
+            finish(step)
+
+        @pl.when((near_step >= 1) & (near_step < half))
+        def _():
+            finish(near_step)
+
+        @pl.when(step == n_ep)
+        def _():
+            finish(0)
 
     def run(t, carry):
         @pl.when((t > 0) & (t < n_ep))
@@ -359,7 +374,7 @@
             from_across(source).wait_recv()
             second(source).start()
 
-        by_urgency(t - 4, pass_across)
+        cross_over(t - 4)
 
         @pl.when((t >= 3) & (t < n_ep + 3))
         def _():
@@ -395,7 +410,7 @@
 
                 attend(block, False)
 
-        by_urgency(t - 5, finish)
+        send_home(t - 5)
 
         done = t - LATER - 2 * row
 
@@ -420,7 +435,7 @@
 
         return carry
 
-    lax.fori_loop(0, n_ep + max(LATER + 1, 5 + 1), run, 0)
+    lax.fori_loop(0, n_ep + LATER + 1, run, 0)
     returned[own] = final[own]
 
     def come_home(step, carry):
@@ -468,6 +483,11 @@
         return carry
 
     lax.fori_loop(0, row_total, drain_kv, 0)
+
+
+def deliver_kernel(mixer_in, expert_in, mixer_out, expert_out):
+    mixer_out[...] = mixer_in[...]
+    expert_out[...] = expert_in[...]
 
 
 def per_device(
@@ -521,7 +541,7 @@
         pltpu.VMEM((4, rows // 4, head_columns), half),
         pltpu.SemaphoreType.DMA((16,)),
     ] + [pair] * 10 + [pltpu.SemaphoreType.DMA((2, 4))]
-    return pl.pallas_call(
+    results = pl.pallas_call(
         functools.partial(fused_kernel, n_ep),
         out_shape=(
             jax.ShapeDtypeStruct((rows // 4, width), half),
@@ -539,6 +559,13 @@
         mixer_post_gain[None], expert_input, expert_ids.T, route_weight.T, expert_gain[None],
         w_gate[0], w_up[0], w_down[0], expert_post_gain[None],
     )
+    return pl.pallas_call(
+        deliver_kernel,
+        out_shape=tuple(jax.ShapeDtypeStruct(part.shape, half) for part in results),
+        in_specs=[vmem, vmem],
+        out_specs=(vmem, vmem),
+        name="deliver",
+    )(*results)
 
 
 def solution(mesh):

time: 71.2 us -> 69.7 us (0.979)
  local copies, waits for them, and re-layouts: 3.55 us -> 0 us
  Pallas kernels: 66.8 us -> 68.9 us
    unnamed x2 -> x0, local copies, waits for them, and re-layouts: 3.55 us -> none
    pallas_call x0 -> x1, Pallas kernels: none -> 2.02 us  [per_device(): pl.pallas_call(deliver_kernel, out_shape=tuple((jax.ShapeDtypeStruct(part...]
where the time goes in v3:
time: 69.7 us; the launch traced here: 69.5 us
  Pallas kernels  68.9 us (99%)
    pallas_call x1, Pallas kernels, per_device(): pl.pallas_call(functools.partial(fused_kernel, n_ep), out_shape=(jax.Shap...  66.8 us
    pallas_call x1, Pallas kernels, per_device(): pl.pallas_call(deliver_kernel, out_shape=tuple((jax.ShapeDtypeStruct(part...  2.02 us

profile of v3, /device:TPU:17, one launch (start us, length us, event | category | flops | bytes accessed | tf_op | source)
XLA Modules:
  0.0 69.5 jit_solution(703465277707657228)
XLA Ops:
  0.6 66.8 %fused.1 = (bf16[128,2048]{1,0:T(8,128)(2,1)}, bf16[64,2048]{1,0:T(8,128)(2,1)}) custom-call(bf16[512,2048]{1,0:T(8,128)(2,1)} %x_hbm.1, f32[4,4096]{1,0:T(4,128)} %gate_hbm.1, f32[1,2048]{1,0:T(1,128)} %bitcast.16, bf16[2048,256]{1,0:T(8,128)(2,1)} %wq_hbm.1, bf16[64,2048]{1,0:T(8,128)(2,1)} %bitcast.14, bf16[64,2048]{1,0:T(8,128)(2,1)} %bitcast.15, ...), custom_call_target="tpu_custom_call" | custom-call | tf_op jit(solution)/shard_map/fused/pallas_call | solution.py:544
  67.5 2.0 %deliver.1 = (bf16[128,2048]{1,0:T(8,128)(2,1)}, bf16[64,2048]{1,0:T(8,128)(2,1)}) custom-call(bf16[128,2048]{1,0:T(8,128)(2,1)} %get-tuple-element.4.mixer_in, bf16[64,2048]{1,0:T(8,128)(2,1)} %get-tuple-element.5.expert_in), custom_call_target="tpu_custom_call" | custom-call | tf_op jit(solution)/shard_map/deliver/pallas_call | solution.py:562

commit v4 on v3

--- a/solution.py
+++ b/solution.py
@@ -348,6 +348,8 @@
         def _():
             finish(0)
 
+    later = LATER
+
     def run(t, carry):
         @pl.when((t > 0) & (t < n_ep))
         def _():
@@ -356,7 +358,7 @@
             to_across(source).start()
             to_beside(source).start()
 
-        early = t - LATER + 2
+        early = t - later + 2
 
         @pl.when((early > 0) & (lax.rem(early + n_ep, 2) == 0) & (early <= 2 * row))
         def _():
@@ -392,13 +394,13 @@
             far(source).start()
             near(source).start()
 
-        @pl.when(t == 2)
+        @pl.when(t == 1)
         def _():
             attend(own, True)
 
-        @pl.when((t > LATER) & (t < n_ep + LATER))
-        def _():
-            turn = t - LATER
+        @pl.when((t > later) & (t < n_ep + later))
+        def _():
+            turn = t - later
 
             @pl.when((turn // 2 <= row) & ((turn > 1) | (column == 1)))
             def _():
@@ -412,9 +414,10 @@
 
         send_home(t - 5)
 
-        done = t - LATER - 2 * row
-
-        @pl.when(done == 1)
+        settled = n_ep + 4
+        ready = later + 2 * row + 1
+
+        @pl.when(((t == ready) & (ready >= settled)) | ((t == settled) & (ready < settled)))
         def _():
             parts = [acc_ref[head, ONES:] / acc_ref[head, 0:1] for head in range(heads)]
             mixed = jnp.concatenate(parts, axis=0).T.astype(jnp.bfloat16)
@@ -485,9 +488,22 @@
     lax.fori_loop(0, row_total, drain_kv, 0)
 
 
-def deliver_kernel(mixer_in, expert_in, mixer_out, expert_out):
-    mixer_out[...] = mixer_in[...]
-    expert_out[...] = expert_in[...]
+def deliver_kernel(mixer_in, expert_in, mixer_out, expert_out, mixer_v, expert_v, sems):
+    taken = (
+        pltpu.make_async_copy(mixer_in, mixer_v, sems.at[0]),
+        pltpu.make_async_copy(expert_in, expert_v, sems.at[1]),
+    )
+    given = (
+        pltpu.make_async_copy(mixer_v, mixer_out, sems.at[2]),
+        pltpu.make_async_copy(expert_v, expert_out, sems.at[3]),
+    )
+    for copy in taken:
+        copy.start()
+    for arrival, departure in zip(taken, given):
+        arrival.wait()
+        departure.start()
+    for copy in given:
+        copy.wait()
 
 
 def per_device(
@@ -562,8 +578,10 @@
     return pl.pallas_call(
         deliver_kernel,
         out_shape=tuple(jax.ShapeDtypeStruct(part.shape, half) for part in results),
-        in_specs=[vmem, vmem],
-        out_specs=(vmem, vmem),
+        in_specs=[far_memory] * 2,
+        out_specs=(far_memory,) * 2,
+        scratch_shapes=[pltpu.VMEM(part.shape, half) for part in results]
+        + [pltpu.SemaphoreType.DMA((4,))],
         name="deliver",
     )(*results)
 

time: 69.7 us -> 69.6 us (level)
  no operation moved by 1% of the time
where the time goes in v4:
time: 69.6 us; the launch traced here: 69.4 us
  Pallas kernels  68.8 us (99%)
    pallas_call x1, Pallas kernels, per_device(): pl.pallas_call(functools.partial(fused_kernel, n_ep), out_shape=(jax.Shap...  66.8 us
    pallas_call x1, Pallas kernels, per_device(): pl.pallas_call(deliver_kernel, out_shape=tuple((jax.ShapeDtypeStruct(part...  1.95 us

profile of v4, /device:TPU:17, one launch (start us, length us, event | category | flops | bytes accessed | tf_op | source)
XLA Modules:
  0.0 69.4 jit_solution(14628678977519326471)
XLA Ops:
  0.6 66.8 %fused.1 = (bf16[128,2048]{1,0:T(8,128)(2,1)}, bf16[64,2048]{1,0:T(8,128)(2,1)}) custom-call(bf16[512,2048]{1,0:T(8,128)(2,1)} %x_hbm.1, f32[4,4096]{1,0:T(4,128)} %gate_hbm.1, f32[1,2048]{1,0:T(1,128)} %bitcast.16, bf16[2048,256]{1,0:T(8,128)(2,1)} %wq_hbm.1, bf16[64,2048]{1,0:T(8,128)(2,1)} %bitcast.14, bf16[64,2048]{1,0:T(8,128)(2,1)} %bitcast.15, ...), custom_call_target="tpu_custom_call" | custom-call | tf_op jit(solution)/shard_map/fused/pallas_call | solution.py:560
  67.5 2.0 %deliver.1 = (bf16[128,2048]{1,0:T(8,128)(2,1)}, bf16[64,2048]{1,0:T(8,128)(2,1)}) custom-call(bf16[128,2048]{1,0:T(8,128)(2,1)} %get-tuple-element.4.mixer_in, bf16[64,2048]{1,0:T(8,128)(2,1)} %get-tuple-element.5.expert_in), custom_call_target="tpu_custom_call" | custom-call | tf_op jit(solution)/shard_map/deliver/pallas_call | solution.py:578
